TPU v7x, 32 devices: a whole 2x2x4 slice. The times are simulated.
32 devices in a mesh: sp: 8 (over z, x), tp: 4 (over y, core).
Axes of the slice: x: 2, y: 2, z: 4, core: 2. Of those that a mesh axis runs over, the one named last changes fastest.
Arguments:
- queries: bfloat16 [3072, 1024], P('sp', 'tp'), may hold values from -160 to 160
- key_vectors: bfloat16 [3072, 1024], P('sp', 'tp'), may hold values from -7 to 7
- values: bfloat16 [3072, 1024], P('sp', 'tp'), may hold values from -6 to 6
- head_lambda: float32 [8], P('tp'), may hold values from 0.3 to 0.8
- head_gain: float32 [128], replicated, may hold values from 0.1 to 1.9
- w_out: bfloat16 [1024, 2048], P('tp'), may hold values from -0.1875 to 0.1875
- residual: bfloat16 [3072, 2048], P(('sp', 'tp')), may hold values from -6 to 6
- ffn_gain: float32 [2048], replicated, may hold values from 0.1 to 1.9
- route_ids: int32 [3072, 2], P(('sp', 'tp')), may hold values from 0 to 7, all different within a row; in each aligned block of 96 rows (0 to 95, 96 to 191, ...) at most 30 rows name the same one
- route_logits: float32 [3072, 2], P(('sp', 'tp')), may hold values from -8 to 310
- w_gate: bfloat16 [8, 2048, 2048], P('sp', None, 'tp'), may hold values from -0.3125 to 0.3125
- w_up: bfloat16 [8, 2048, 2048], P('sp', None, 'tp'), may hold values from -0.3125 to 0.3125
- w_down: bfloat16 [8, 2048, 2048], P('sp', 'tp'), may hold values from -0.125 to 0.125
Outputs:
- layer_out: bfloat16 [3072, 2048], P(('sp', 'tp'))
Inputs may be any that keep to these rules, and one draw needn't show every extreme that they name: `route_ids`: in the rows of one device after the attention (aligned blocks of 96 rows) no expert is named by more than 30 rows, a bound that some block reaches while other experts in the same block get fewer rows; each row names 2 different experts.
All inputs are finite; a program needn't handle non-finite values.
Results may differ from a plain program's by a relative error of at most 0.023.
Values may be sent and summed in bfloat16 or wider, within the bound.
A program may use at most 192 MiB of HBM per device.

v0:
```python
import jax
import jax.numpy as jnp
from jax import lax
from jax.sharding import PartitionSpec as P

SEGMENT = 64
SEQUENCES = 1
EPS = 1e-06
NEG = -1e30
CLAMP = 7.0
ALPHA = 1.702
OUT_FACTOR = 0.8


def shards(
    queries,
    key_vectors,
    values,
    head_lambda,
    head_gain,
    w_out,
    residual,
    ffn_gain,
    route_ids,
    route_logits,
    w_gate,
    w_up,
    w_down,
):
    tok_count = queries.shape[0]
    local_heads = head_lambda.shape[0]
    head_width = queries.shape[1] // (2 * local_heads)
    value_width = values.shape[1] // local_heads
    score_scale = head_width ** (-0.5)
    n_tp = lax.axis_size("tp")
    n_sp = lax.axis_size("sp")
    seq_length = tok_count * n_sp // SEQUENCES
    query_pos = lax.axis_index("sp") * tok_count + jnp.arange(tok_count, dtype=jnp.int32)
    query_seg = query_pos // SEGMENT
    query_seq = query_pos // seq_length
    seq_begin = query_seq[0] * seq_length
    last_seg = query_seg[tok_count - 1]
    query_heads = queries.reshape(tok_count, local_heads, 2, head_width)

    def absorb(carry, key_block, value_block, key_start):
        maxima, totals, sums = carry
        block_len = key_block.shape[0]
        key_pos = key_start + jnp.arange(block_len, dtype=jnp.int32)
        visible = ((key_pos // SEGMENT)[None, :] <= query_seg[:, None]) & (
            (key_pos // seq_length)[None, :] == query_seq[:, None]
        )
        score = (
            jnp.einsum(
                "qhjd,khjd->jhqk", query_heads, key_block, preferred_element_type=jnp.float32
            )
            * score_scale
        )
        score = jnp.where(visible, score, NEG)
        new_max = jnp.maximum(maxima, jnp.max(score, axis=-1))
        expo = jnp.where(visible, jnp.exp(score - new_max[..., None]), 0.0)
        factor = jnp.exp(maxima - new_max)
        totals = totals * factor + jnp.sum(expo, axis=-1)
        added = jnp.einsum(
            "jhqk,khd->jqhd",
            expo.astype(jnp.bfloat16),
            value_block,
            preferred_element_type=jnp.float32,
        )
        sums = sums * jnp.transpose(factor, (0, 2, 1))[..., None] + added
        return (new_max, totals, sums)

    def maybe_absorb(carry, key_block, value_block, key_start):
        block_len = key_block.shape[0]
        needed = (key_start // SEGMENT <= last_seg) & (key_start + block_len - 1 >= seq_begin)
        return lax.cond(
            needed,
            lambda inner: absorb(inner, key_block, value_block, key_start),
            lambda inner: inner,
            carry,
        )

    initial = (
        jnp.full((2, local_heads, tok_count), NEG, jnp.float32),
        jnp.zeros((2, local_heads, tok_count), jnp.float32),
        jnp.zeros((2, tok_count, local_heads, value_width), jnp.float32),
    )
    key_piece = lax.all_gather(key_vectors, "sp", axis=0, tiled=True)
    value_piece = lax.all_gather(values, "sp", axis=0, tiled=True)
    piece_len = key_piece.shape[0]
    key_rows = key_piece.reshape(piece_len, local_heads, 2, head_width)
    value_rows = value_piece.reshape(piece_len, local_heads, value_width)
    key_step = 512

    def advance(block_index, inner):
        key_offset = block_index * key_step
        key_block = lax.dynamic_slice_in_dim(key_rows, key_offset, key_step, 0)
        value_block = lax.dynamic_slice_in_dim(value_rows, key_offset, key_step, 0)
        return maybe_absorb(inner, key_block, value_block, key_offset)

    maxima, totals, sums = lax.fori_loop(0, piece_len // key_step, advance, initial)
    attended = sums / jnp.transpose(totals, (0, 2, 1))[..., None]
    diff = attended[0] - head_lambda[None, :, None] * attended[1]
    scale_rows = lax.rsqrt(jnp.mean(diff * diff, axis=-1, keepdims=True) + EPS)
    head_rows = (diff * scale_rows * head_gain * OUT_FACTOR).astype(jnp.bfloat16)
    head_rows = head_rows.reshape(tok_count, local_heads * value_width)
    own_count = tok_count // n_tp
    whole_weight = lax.all_gather(w_out, "tp", axis=0, tiled=True)
    token_heads = lax.all_to_all(head_rows, "tp", split_axis=0, concat_axis=1, tiled=True)
    projected = jnp.dot(token_heads, whole_weight, preferred_element_type=jnp.float32)
    mixed = (residual.astype(jnp.float32) + projected).astype(jnp.bfloat16)
    mixed32 = mixed.astype(jnp.float32)
    normed = (
        mixed32 * lax.rsqrt(jnp.mean(mixed32 * mixed32, axis=-1, keepdims=True) + EPS) * ffn_gain
    ).astype(jnp.bfloat16)
    gates = jax.nn.softmax(route_logits, axis=-1)
    top_count = route_ids.shape[1]
    model_width = normed.shape[1]
    cap_slots = max(2, 5 * top_count * tok_count // (4 * n_tp * n_sp))
    flat_ids = route_ids.reshape(-1)
    chosen = (flat_ids[:, None] == jnp.arange(n_sp, dtype=jnp.int32)[None, :]).astype(jnp.int32)
    earlier = jnp.cumsum(chosen, axis=0) - chosen
    slot_rank = jnp.sum(earlier * chosen, axis=1)
    slot_index = flat_ids * cap_slots + slot_rank
    source_rows = jnp.repeat(normed, top_count, axis=0)
    outgoing = (
        jnp.zeros((n_sp * cap_slots, model_width), jnp.bfloat16).at[slot_index].set(source_rows)
    )
    outgoing = outgoing.reshape(n_sp, cap_slots, model_width)
    arrived = lax.all_to_all(outgoing, "sp", split_axis=0, concat_axis=0, tiled=True)
    senders, slot_count, arrived_width = arrived.shape
    flat_in = arrived.reshape(senders * slot_count, arrived_width)
    piece = lax.all_gather(flat_in, "tp", axis=0, tiled=True)
    gate_pre = jnp.dot(piece, w_gate[0], preferred_element_type=jnp.float32)
    up_pre = jnp.dot(piece, w_up[0], preferred_element_type=jnp.float32)
    gate_cut = jnp.minimum(gate_pre, CLAMP)
    up_cut = jnp.clip(up_pre, -CLAMP, CLAMP)
    active = (gate_cut * jax.nn.sigmoid(ALPHA * gate_cut) * (up_cut + 1.0)).astype(jnp.bfloat16)
    reduced = lax.psum_scatter(
        jnp.dot(active, w_down[0], preferred_element_type=jnp.float32).astype(jnp.bfloat16),
        "tp",
        scatter_dimension=0,
        tiled=True,
    )
    reduced = reduced.reshape(senders, slot_count, arrived_width)
    returned = lax.all_to_all(reduced, "sp", split_axis=0, concat_axis=0, tiled=True)
    picked = returned.reshape(n_sp * cap_slots, model_width)[slot_index].astype(jnp.float32)
    weighted = (picked * gates.reshape(-1)[:, None]).reshape(own_count, top_count, model_width)
    return (mixed32 + jnp.sum(weighted, axis=1)).astype(jnp.bfloat16)


def solution(mesh):
    in_specs = (
        P("sp", "tp"),
        P("sp", "tp"),
        P("sp", "tp"),
        P("tp"),
        P(),
        P("tp", None),
        P(("sp", "tp"), None),
        P(),
        P(("sp", "tp"), None),
        P(("sp", "tp"), None),
        P("sp", None, "tp"),
        P("sp", None, "tp"),
        P("sp", "tp", None),
    )
    out_specs = P(("sp", "tp"), None)
    return jax.shard_map(shards, mesh=mesh, in_specs=in_specs, out_specs=out_specs, check_vma=False)
```

profile of v0, /device:TPU:0, one launch (start us, length us, event | category | flops | bytes accessed | tf_op | source)
XLA Modules:
  0.0 338.7 jit_solution(3574506045380296739)
XLA Ops:
  6.6 1.9 copy.37
  14.6 42.0 %all-gather.5.cloned.1.call-done = bf16[3072,256]{0,1:T(8,128)(2,1)} async-done(((bf16[384,256]{0,1:T(8,128)(2,1)}), bf16[3072,256]{0,1:T(8,128)(2,1)}) %all-gather.5.cloned.1.call-update) | async-done | bytes 1572880 | tf_op jit(solution)/shard_map/all_gather | solution.py:87
  56.6 2.7 copy.40
  59.3 42.0 %all-gather.7.cloned.1.call-done = bf16[3072,256]{0,1:T(8,128)(2,1)} async-done(((bf16[384,256]{0,1:T(8,128)(2,1)}), bf16[3072,256]{0,1:T(8,128)(2,1)}) %all-gather.7.cloned.1.call-update) | async-done | bytes 1572880 | tf_op jit(solution)/shard_map/all_gather | solution.py:88
  101.3 2.6 copy.42
  104.0 9.5 %while.24 = (s32[]{:T(128)}, f32[2,2,384]{2,1,0:T(2,128)S(1)}, f32[2,2,384]{2,1,0:T(2,128)S(1)}, f32[2,384,2,128]{3,1,0,2:T(8,128)S(1)}, s32[]{:T(128)}, /*index...) while((s32[]{:T(128)}, f32[2,2,384]{2,1,0:T(2,128)S(1)}, ...), condition=%wide.region_5.6_spmd.clone.clone, body=%wide.region_0.5_spmd.clone.clone.sunk | while | flops 310077472 | bytes 12468234 | solution.py:100
  104.7 4.9 %conditional.4 = ((f32[2,2,384]{2,1,0:T(2,128)S(1)}, f32[2,2,384]{2,1,0:T(2,128)S(1)}, f32[2,384,2,128]{3,1,0,2:T(8,128)S(1)})) conditional(s32[]{:T(128)} %convert_element_type.87, (f32[2,2,384]{2,1,0:T(2,128)S(1)}, f32[2,2,384]{2,1,0:T(2,128)S(1)}, f32[2,384,2,128]{3,1,0,2:T(8,128)S(1)}) %tuple.101, (s32[]{:T(128)}, ...), branch_computations={%region_1.1_spmd, %region_2.4_spmd.clone} | conditional | flops 310070912 | bytes 12456133 | solution.py:75
  122.2 3.4 all-to-all-start
  125.6 7.7 %all-to-all-done = bf16[4,96,256]{2,1,0:T(8,128)(2,1)S(1)} async-done(((bf16[4,96,256]{2,1,0:T(8,128)(2,1)}), bf16[4,96,256]{2,1,0:T(8,128)(2,1)S(1)}, u32[]{:S(2)}, u32[]{:S(2)}) %all-to-all-start) | async-done | bytes 196640 | tf_op jit(solution)/shard_map/all_to_all | solution.py:108
  133.3 4.3 %all-gather.9.cloned.1.call-done = bf16[1024,2048]{1,0:T(8,128)(2,1)} async-done(((bf16[256,2048]{1,0:T(8,128)(2,1)}), bf16[1024,2048]{1,0:T(8,128)(2,1)}) %all-gather.9.cloned.1.call-update) | async-done | bytes 4194320 | tf_op jit(solution)/shard_map/all_gather | solution.py:107
  137.6 3.2 multiply_reduce_fusion.1
  143.6 3.3 scatter_custom_fusion
  148.4 45.5 %all_to_all.26 = bf16[8,30,2048]{2,1,0:T(8,128)(2,1)} all-to-all(bf16[8,30,2048]{2,1,0:T(8,128)(2,1)S(1)} %reshape.158), channel_id=1, replica_groups=mesh['sp'=8,'tp'=4] {'sp'}, dimensions={0} | all-to-all | bytes 1966080 | tf_op jit(solution)/shard_map/all_to_all | solution.py:129
  193.9 2.4 reshape.159
  196.6 31.4 %all-gather.11.cloned.1.call-done = bf16[960,2048]{1,0:T(8,128)(2,1)} async-done(((bf16[240,2048]{1,0:T(8,128)(2,1)}), bf16[960,2048]{1,0:T(8,128)(2,1)}) %all-gather.11.cloned.1.call-update) | async-done | bytes 3932176 | tf_op jit(solution)/shard_map/all_gather | solution.py:132
  228.0 6.3 %fusion.35 = f32[960,512]{1,0:T(8,128)} fusion(bf16[960,2048]{1,0:T(8,128)(2,1)} %all-gather.11.cloned.1.call-done, bf16[1,2048,512]{2,1,0:T(8,128)(2,1)} %param.28), kind=kOutput, calls=%fused_computation.54 | convolution fusion | flops 2013265920 | bytes 7995392 | tf_op jit(solution)/shard_map/dot_general | solution.py:134
  234.4 9.8 %convolution_convert_fusion = bf16[960,2048]{1,0:T(8,128)(2,1)} fusion(bf16[1,512,2048]{2,1,0:T(8,128)(2,1)S(1)} %copy-done, f32[960,512]{1,0:T(8,128)} %fusion.35, bf16[960,2048]{1,0:T(8,128)(2,1)} %all-gather.11.cloned.1.call-done, bf16[1,2048,512]{2,1,0:T(8,128)(2,1)} %param.27), kind=kOutput, calls=%fused_computation.49 | convolution fusion | flops 4033413120 | bytes 14024704 | tf_op jit(solution)/shard_map/dot_general | solution.py:139
  244.3 43.0 %reduce-scatter.2.cloned.1.call-done = bf16[240,2048]{1,0:T(8,128)(2,1)} async-done(((bf16[960,2048]{1,0:T(8,128)(2,1)}), bf16[240,2048]{1,0:T(8,128)(2,1)}) %reduce-scatter.2.cloned.1.call-update) | async-done | bytes 983056 | tf_op jit(solution)/shard_map/reduce_scatter | solution.py:138
  287.3 2.4 reshape.160
  289.7 5.5 %all-to-all-start.2 = ((bf16[8,30,2048]{2,1,0:T(8,128)(2,1)}), bf16[8,30,2048]{2,1,0:T(8,128)(2,1)}, u32[]{:S(2)}, u32[]{:S(2)}) async-start(bf16[8,30,2048]{2,1,0:T(8,128)(2,1)} %reshape.160), calls=%async_computation.3 | async-start | bytes 2097152 | tf_op jit(solution)/shard_map/all_to_all | solution.py:145
  295.4 25.6 %all-to-all-done.2 = bf16[8,30,2048]{2,1,0:T(8,128)(2,1)} async-done(((bf16[8,30,2048]{2,1,0:T(8,128)(2,1)}), bf16[8,30,2048]{2,1,0:T(8,128)(2,1)}, u32[]{:S(2)}, u32[]{:S(2)}) %all-to-all-start.2) | async-done | bytes 983072 | tf_op jit(solution)/shard_map/all_to_all | solution.py:145
  322.5 2.0 gather_fusion
  324.5 3.0 reshape.163
  327.6 3.7 %multiply_reduce_fusion = f32[96,2048]{1,0:T(8,128)S(1)} fusion(f32[96,2,2048]{2,1,0:T(2,128)} %reshape.163, f32[96,2]{1,0:T(8,128)S(1)} %copy.51), kind=kLoop, calls=%fused_computation.59 | loop fusion | flops 589824 | bytes 2360064 | tf_op jit(solution)/shard_map/reduce_sum | solution.py:148
  (135 shorter events, 26.3 us)
Async XLA Ops:
  6.5 227.8 %copy-start = (bf16[1,512,2048]{2,1,0:T(8,128)(2,1)S(1)}, bf16[1,512,2048]{2,1,0:T(8,128)(2,1)}, u32[]{:S(2)}) copy-start(bf16[1,512,2048]{2,1,0:T(8,128)(2,1)} %param.29) | copy-start | bytes 6291460
  6.5 5.7 %copy-start.6 = (bf16[384,256]{1,0:T(8,128)(2,1)S(1)}, bf16[384,256]{1,0:T(8,128)(2,1)}, u32[]{:S(2)}) copy-start(bf16[384,256]{1,0:T(8,128)(2,1)} %param.17) | copy-start | bytes 589828
  6.5 5.9 %copy-start.9 = (s32[96,2]{0,1:T(2,128)S(1)}, s32[96,2]{0,1:T(2,128)}, u32[]{:S(2)}) copy-start(s32[96,2]{0,1:T(2,128)} %param.25) | copy-start | bytes 2308
  6.5 8.0 %copy-start.10 = (f32[2]{0:T(128)S(1)}, f32[2]{0:T(128)}, u32[]{:S(2)}) copy-start(f32[2]{0:T(128)} %param.20) | copy-start | bytes 28
  6.5 8.0 %copy-start.11 = (f32[128]{0:T(128)S(1)}, f32[128]{0:T(128)}, u32[]{:S(2)}) copy-start(f32[128]{0:T(128)} %param.21) | copy-start | bytes 1540
  6.5 50.0 %all-gather.5.cloned.1.call-start = ((), (), s32[]{:S(2)}) async-start(), calls=%async_computation.4 | async-start | bytes 1769472 | tf_op jit(solution)/shard_map/all_gather | solution.py:87
  8.5 92.8 %all-gather.7.cloned.1.call-start = ((), (), s32[]{:S(2)}) async-start(), calls=%async_computation.5 | async-start | bytes 1769472 | tf_op jit(solution)/shard_map/all_gather | solution.py:88
  10.3 127.3 %all-gather.9.cloned.1.call-start = ((), (), s32[]{:S(2)}) async-start(), calls=%async_computation.6 | async-start | bytes 5242880 | tf_op jit(solution)/shard_map/all_gather | solution.py:107
  113.7 0.9 copy-start.1
  115.4 3.8 %copy-start.2 = (f32[2,384,2,128]{3,1,0,2:T(8,128)S(1)}, f32[2,384,2,128]{3,1,0,2:T(8,128)}, u32[]{:S(2)}) copy-start(f32[2,384,2,128]{3,1,0,2:T(8,128)} %copy-done.1) | copy-start | bytes 2359300
  119.2 1.2 copy-start.5
  122.2 11.2 %all-to-all-start = ((bf16[4,96,256]{2,1,0:T(8,128)(2,1)}), bf16[4,96,256]{2,1,0:T(8,128)(2,1)S(1)}, u32[]{:S(2)}, u32[]{:S(2)}) async-start(bf16[4,96,256]{2,1,0:T(8,128)(2,1)} %multiply_convert_fusion.2), calls=%async_computation | async-start | bytes 393216 | tf_op jit(solution)/shard_map/all_to_all | solution.py:108
  125.5 102.5 %all-gather.11.cloned.1.call-start = ((), (), s32[]{:S(2)}) async-start(), calls=%async_computation.7 | async-start | bytes 4915200 | tf_op jit(solution)/shard_map/all_gather | solution.py:132
  137.6 4.1 %copy-start.8 = (f32[2048]{0:T(1024)S(1)}, f32[2048]{0:T(1024)}, u32[]{:S(2)}) copy-start(f32[2048]{0:T(1024)} %param.24) | copy-start | bytes 24580
  140.8 0.9 copy-start.3
  196.4 90.9 %reduce-scatter.2.cloned.1.call-start = ((), (), s32[]{:S(2)}) async-start(), calls=%async_computation.8 | async-start | bytes 4915200 | tf_op jit(solution)/shard_map/reduce_scatter | solution.py:138
  244.2 51.0 %copy-start.7 = (f32[96,2]{0,1:T(2,128)S(1)}, f32[96,2]{0,1:T(2,128)}, u32[]{:S(2)}) copy-start(f32[96,2]{0,1:T(2,128)} %param.26) | copy-start | bytes 2308
  289.7 31.3 %all-to-all-start.2 = ((bf16[8,30,2048]{2,1,0:T(8,128)(2,1)}), bf16[8,30,2048]{2,1,0:T(8,128)(2,1)}, u32[]{:S(2)}, u32[]{:S(2)}) async-start(bf16[8,30,2048]{2,1,0:T(8,128)(2,1)} %reshape.160), calls=%async_computation.3 | async-start | bytes 2097152 | tf_op jit(solution)/shard_map/all_to_all | solution.py:145
  324.5 6.8 %copy-start.4 = (f32[96,2048]{1,0:T(8,128)S(1)}, f32[96,2048]{1,0:T(8,128)}, u32[]{:S(2)}) copy-start(f32[96,2048]{1,0:T(8,128)} %copy-done.3) | copy-start | bytes 2359300
Sparse Core Ops, SparseCore 0:
  9.4 47.1 all-gather.4
  58.6 42.5 all-gather.6
  102.9 34.7 all-gather.8
  196.5 31.4 all-gather.10
  244.4 42.8 reduce-scatter.1
where the time goes:
time: 340 us; the launch traced here: 339 us
  waiting for transfers between devices  197 us (58%)
  blocking collectives  45.5 us (13%)
  local copies, waits for them, and re-layouts  36.4 us (11%)
  matrix products  22.9 us (7%)
  between operations  14.1 us (4%)
  starting transfers between devices  9.27 us (3%)
  other arithmetic  9.27 us (3%)
  loops' own time  4.41 us (1%)
    all_to_all x1, blocking collectives, shards(): lax.all_to_all(outgoing, 'sp', split_axis=0, concat_axis=0, tiled=True)  45.5 us
    reduce_scatter x1, waiting for transfers between devices, shards(): lax.psum_scatter(jnp.dot(active, w_down[0], preferred_element_type=jnp.fl...  43 us
    all_gather x1, waiting for transfers between devices, shards(): value_piece = lax.all_gather(values, 'sp', axis=0, tiled=True)  42 us
    all_gather x1, waiting for transfers between devices, shards(): key_piece = lax.all_gather(key_vectors, 'sp', axis=0, tiled=True)  42 us
    all_gather x1, waiting for transfers between devices, shards(): piece = lax.all_gather(flat_in, 'tp', axis=0, tiled=True)  31.4 us
    all_to_all x1, waiting for transfers between devices, shards(): lax.all_to_all(reduced, 'sp', split_axis=0, concat_axis=0, tiled=True)  25.6 us
    unnamed x31, local copies, waits for them, and re-layouts  11 us
    dot_general x1, matrix products, shards(): jnp.dot(active, w_down[0], preferred_element_type=jnp.float32)  9.84 us
  transfers between devices with their start and end apart: 7, of which 7 were waited for; matrix products, arithmetic and copies ran while one was open for 7% of the time, Pallas kernels for 0%

commit v1 on v0

--- a/solution.py
+++ b/solution.py
@@ -10,6 +10,11 @@
 CLAMP = 7.0
 ALPHA = 1.702
 OUT_FACTOR = 0.8
+_hold_matrix = lambda vals, local_array, axis_name: jnp.split(
+    lax.all_gather(jnp.concatenate([vals, local_array], axis=1), axis_name, axis=0, tiled=True),
+    [vals.shape[1]],
+    axis=1,
+)
 
 
 def shards(
@@ -84,8 +89,7 @@
         jnp.zeros((2, local_heads, tok_count), jnp.float32),
         jnp.zeros((2, tok_count, local_heads, value_width), jnp.float32),
     )
-    key_piece = lax.all_gather(key_vectors, "sp", axis=0, tiled=True)
-    value_piece = lax.all_gather(values, "sp", axis=0, tiled=True)
+    key_piece, value_piece = _hold_matrix(key_vectors, values, "sp")
     piece_len = key_piece.shape[0]
     key_rows = key_piece.reshape(piece_len, local_heads, 2, head_width)
     value_rows = value_piece.reshape(piece_len, local_heads, value_width)

time: 340 us -> 318 us (0.935)
  waiting for transfers between devices: 197 us -> 168 us
  blocking collectives: 45.5 us -> 51.1 us
    all_gather x2 -> x1, waiting for transfers between devices: 84 us -> 61.2 us  [lax.all_gather(jnp.concatenate([vals, local_array], axis=1), axis_name, a...]
    all_to_all x1, blocking collectives: 45.5 us -> 51.1 us  [shards(): lax.all_to_all(outgoing, 'sp', split_axis=0, concat_axis=0, tiled=True)]
    all_gather x1, waiting for transfers between devices: 4.3 us -> 0.38 us  [shards(): whole_weight = lax.all_gather(w_out, 'tp', axis=0, tiled=True)]
  transfers between devices with their start and end apart: 7 -> 6, of which waited for: 7 -> 6; matrix products, arithmetic and copies ran while one was open for 7% -> 7% of each run, Pallas kernels for 0% -> 0%
where the time goes in v1:
time: 318 us; the launch traced here: 317 us
  waiting for transfers between devices  168 us (53%)
  blocking collectives  51.1 us (16%)
  local copies, waits for them, and re-layouts  37.1 us (12%)
  matrix products  22.9 us (7%)
  between operations  14.1 us (4%)
  other arithmetic  10.1 us (3%)
  starting transfers between devices  9.22 us (3%)
  loops' own time  4.1 us (1%)
    all_gather x1, waiting for transfers between devices, lax.all_gather(jnp.concatenate([vals, local_array], axis=1), axis_name, a...  61.2 us
    all_to_all x1, blocking collectives, shards(): lax.all_to_all(outgoing, 'sp', split_axis=0, concat_axis=0, tiled=True)  51.1 us
    reduce_scatter x1, waiting for transfers between devices, shards(): lax.psum_scatter(jnp.dot(active, w_down[0], preferred_element_type=jnp.fl...  43 us
    all_gather x1, waiting for transfers between devices, shards(): piece = lax.all_gather(flat_in, 'tp', axis=0, tiled=True)  31.4 us
    all_to_all x1, waiting for transfers between devices, shards(): lax.all_to_all(reduced, 'sp', split_axis=0, concat_axis=0, tiled=True)  25.6 us
    dot_general x1, matrix products, shards(): jnp.dot(active, w_down[0], preferred_element_type=jnp.float32)  9.85 us
    unnamed x31, local copies, waits for them, and re-layouts  8.37 us
  transfers between devices with their start and end apart: 6, of which 6 were waited for; matrix products, arithmetic and copies ran while one was open for 7% of the time, Pallas kernels for 0%

profile of v1, /device:TPU:0, one launch (start us, length us, event | category | flops | bytes accessed | tf_op | source)
XLA Modules:
  0.0 317.0 jit_solution(3674973550278679588)
XLA Ops:
  14.1 61.2 %all-gather.4.cloned.1.call-done = bf16[3072,512]{0,1:T(8,128)(2,1)} async-done(((bf16[384,512]{0,1:T(8,128)(2,1)}), bf16[3072,512]{0,1:T(8,128)(2,1)}) %all-gather.4.cloned.1.call-update) | async-done | bytes 3145744 | tf_op jit(solution)/shard_map/all_gather | solution.py:14
  75.3 3.3 %fusion.59 = (bf16[3072,256]{0,1:T(8,128)(2,1)}, bf16[3072,256]{0,1:T(8,128)(2,1)S(1)}) fusion(bf16[3072,512]{0,1:T(8,128)(2,1)} %all-gather.4.cloned.1.call-done), kind=kLoop, calls=%fused_computation.107 | loop fusion | bytes 6291456 | tf_op jit(solution)/shard_map/split | solution.py:13
  79.9 2.7 copy.42
  82.6 9.2 %while.24 = (s32[]{:T(128)}, f32[2,2,384]{2,1,0:T(2,128)S(1)}, f32[2,2,384]{2,1,0:T(2,128)S(1)}, f32[2,384,2,128]{3,1,0,2:T(8,128)S(1)}, s32[]{:T(128)}, /*index...) while((s32[]{:T(128)}, f32[2,2,384]{2,1,0:T(2,128)S(1)}, ...), condition=%wide.region_5.6_spmd.clone.clone, body=%wide.region_0.5_spmd.clone.clone.sunk | while | flops 310077472 | bytes 12468234 | solution.py:104
  83.3 4.9 %conditional.4 = ((f32[2,2,384]{2,1,0:T(2,128)S(1)}, f32[2,2,384]{2,1,0:T(2,128)S(1)}, f32[2,384,2,128]{3,1,0,2:T(8,128)S(1)})) conditional(s32[]{:T(128)} %convert_element_type.87, (f32[2,2,384]{2,1,0:T(2,128)S(1)}, f32[2,2,384]{2,1,0:T(2,128)S(1)}, f32[2,384,2,128]{3,1,0,2:T(8,128)S(1)}) %tuple.102, (s32[]{:T(128)}, ...), branch_computations={%region_1.1_spmd, %region_2.4_spmd.clone} | conditional | flops 310070912 | bytes 12456133 | solution.py:80
  83.7 1.7 fusion.4
  86.4 1.9 fusion.12
  98.8 1.8 multiply_convert_fusion.2
  100.5 3.4 %all-to-all-start = ((bf16[4,96,256]{2,1,0:T(8,128)(2,1)}), bf16[4,96,256]{2,1,0:T(8,128)(2,1)S(1)}, u32[]{:S(2)}, u32[]{:S(2)}) async-start(bf16[4,96,256]{2,1,0:T(8,128)(2,1)} %multiply_convert_fusion.2), calls=%async_computation | async-start | bytes 393216 | tf_op jit(solution)/shard_map/all_to_all | solution.py:112
  104.0 6.0 %all-to-all-done = bf16[4,96,256]{2,1,0:T(8,128)(2,1)S(1)} async-done(((bf16[4,96,256]{2,1,0:T(8,128)(2,1)}), bf16[4,96,256]{2,1,0:T(8,128)(2,1)S(1)}, u32[]{:S(2)}, u32[]{:S(2)}) %all-to-all-start) | async-done | bytes 196640 | tf_op jit(solution)/shard_map/all_to_all | solution.py:112
  110.4 3.2 %multiply_reduce_fusion.1 = (f32[96]{0:T(128)S(1)}, f32[96,2048]{1,0:T(8,128)S(1)}) fusion(bf16[96,1024]{1,0:T(8,128)(2,1)S(1)} %bitcast.79, bf16[1024,2048]{1,0:T(8,128)(2,1)} %all-gather.6.cloned.1.call-done, bf16[96,2048]{1,0:T(8,128)(2,1)} %param.23), kind=kOutput, calls=%fused_computation.62 | convolution fusion | flops 403832736 | bytes 5570944 | tf_op jit(solution)/shard_map/dot_general | solution.py:113
  116.3 3.3 %scatter_custom_fusion = bf16[240,2048]{1,0:T(8,128)(2,1)} fusion(s32[192]{0:T(256)S(1)} %bitcast.84, bf16[192,2048]{1,0:T(8,128)(2,1)} %reshape.176, bf16[]{:T(256)} %constant.234.clone.1), kind=kCustom, calls=%fused_computation.63 | custom fusion | bytes 983552 | tf_op jit(solution)/shard_map/scatter | solution.py:130
  121.2 51.1 %all_to_all.26 = bf16[8,30,2048]{2,1,0:T(8,128)(2,1)} all-to-all(bf16[8,30,2048]{2,1,0:T(8,128)(2,1)S(1)} %reshape.158), channel_id=1, replica_groups=mesh['sp'=8,'tp'=4] {'sp'}, dimensions={0} | all-to-all | bytes 1966080 | tf_op jit(solution)/shard_map/all_to_all | solution.py:133
  172.3 2.4 reshape.159
  175.0 31.4 %all-gather.8.cloned.1.call-done = bf16[960,2048]{1,0:T(8,128)(2,1)} async-done(((bf16[240,2048]{1,0:T(8,128)(2,1)}), bf16[960,2048]{1,0:T(8,128)(2,1)}) %all-gather.8.cloned.1.call-update) | async-done | bytes 3932176 | tf_op jit(solution)/shard_map/all_gather | solution.py:136
  206.4 6.3 %fusion.35 = f32[960,512]{1,0:T(8,128)} fusion(bf16[960,2048]{1,0:T(8,128)(2,1)} %all-gather.8.cloned.1.call-done, bf16[1,2048,512]{2,1,0:T(8,128)(2,1)} %param.28), kind=kOutput, calls=%fused_computation.54 | convolution fusion | flops 2013265920 | bytes 7995392 | tf_op jit(solution)/shard_map/dot_general | solution.py:138
  212.7 9.8 %convolution_convert_fusion = bf16[960,2048]{1,0:T(8,128)(2,1)} fusion(bf16[1,512,2048]{2,1,0:T(8,128)(2,1)S(1)} %copy-done, f32[960,512]{1,0:T(8,128)} %fusion.35, bf16[960,2048]{1,0:T(8,128)(2,1)} %all-gather.8.cloned.1.call-done, bf16[1,2048,512]{2,1,0:T(8,128)(2,1)} %param.27), kind=kOutput, calls=%fused_computation.49 | convolution fusion | flops 4033413120 | bytes 14024704 | tf_op jit(solution)/shard_map/dot_general | solution.py:143
  222.6 43.0 %reduce-scatter.2.cloned.1.call-done = bf16[240,2048]{1,0:T(8,128)(2,1)} async-done(((bf16[960,2048]{1,0:T(8,128)(2,1)}), bf16[240,2048]{1,0:T(8,128)(2,1)}) %reduce-scatter.2.cloned.1.call-update) | async-done | bytes 983056 | tf_op jit(solution)/shard_map/reduce_scatter | solution.py:142
  265.6 2.4 reshape.160
  268.0 5.5 %all-to-all-start.2 = ((bf16[8,30,2048]{2,1,0:T(8,128)(2,1)}), bf16[8,30,2048]{2,1,0:T(8,128)(2,1)}, u32[]{:S(2)}, u32[]{:S(2)}) async-start(bf16[8,30,2048]{2,1,0:T(8,128)(2,1)} %reshape.160), calls=%async_computation.3 | async-start | bytes 2097152 | tf_op jit(solution)/shard_map/all_to_all | solution.py:149
  273.7 25.6 %all-to-all-done.2 = bf16[8,30,2048]{2,1,0:T(8,128)(2,1)} async-done(((bf16[8,30,2048]{2,1,0:T(8,128)(2,1)}), bf16[8,30,2048]{2,1,0:T(8,128)(2,1)}, u32[]{:S(2)}, u32[]{:S(2)}) %all-to-all-start.2) | async-done | bytes 983072 | tf_op jit(solution)/shard_map/all_to_all | solution.py:149
  300.8 2.0 gather_fusion
  302.9 3.0 reshape.163
  305.9 3.7 %multiply_reduce_fusion = f32[96,2048]{1,0:T(8,128)S(1)} fusion(f32[96,2,2048]{2,1,0:T(2,128)} %reshape.163, f32[96,2]{1,0:T(8,128)S(1)} %copy.51), kind=kLoop, calls=%fused_computation.59 | loop fusion | flops 589824 | bytes 2360064 | tf_op jit(solution)/shard_map/reduce_sum | solution.py:152
  (134 shorter events, 24.0 us)
Async XLA Ops:
  6.5 206.2 %copy-start = (bf16[1,512,2048]{2,1,0:T(8,128)(2,1)S(1)}, bf16[1,512,2048]{2,1,0:T(8,128)(2,1)}, u32[]{:S(2)}) copy-start(bf16[1,512,2048]{2,1,0:T(8,128)(2,1)} %param.29) | copy-start | bytes 6291460
  6.5 5.1 %copy-start.6 = (bf16[384,256]{1,0:T(8,128)(2,1)S(1)}, bf16[384,256]{1,0:T(8,128)(2,1)}, u32[]{:S(2)}) copy-start(bf16[384,256]{1,0:T(8,128)(2,1)} %param.17) | copy-start | bytes 589828
  6.5 5.3 %copy-start.9 = (s32[96,2]{0,1:T(2,128)S(1)}, s32[96,2]{0,1:T(2,128)}, u32[]{:S(2)}) copy-start(s32[96,2]{0,1:T(2,128)} %param.25) | copy-start | bytes 2308
  6.5 7.5 %copy-start.10 = (f32[2]{0:T(128)S(1)}, f32[2]{0:T(128)}, u32[]{:S(2)}) copy-start(f32[2]{0:T(128)} %param.20) | copy-start | bytes 28
  6.5 7.5 %copy-start.11 = (f32[128]{0:T(128)S(1)}, f32[128]{0:T(128)}, u32[]{:S(2)}) copy-start(f32[128]{0:T(128)} %param.21) | copy-start | bytes 1540
  6.5 68.7 %all-gather.4.cloned.1.call-start = ((), (), s32[]{:S(2)}) async-start(), calls=%async_computation.4 | async-start | bytes 3538944 | tf_op jit(solution)/shard_map/all_gather | solution.py:14
  9.7 100.7 %all-gather.6.cloned.1.call-start = ((), (), s32[]{:S(2)}) async-start(), calls=%async_computation.5 | async-start | bytes 5242880 | tf_op jit(solution)/shard_map/all_gather | solution.py:111
  92.1 0.9 copy-start.1
  93.8 3.7 %copy-start.2 = (f32[2,384,2,128]{3,1,0,2:T(8,128)S(1)}, f32[2,384,2,128]{3,1,0,2:T(8,128)}, u32[]{:S(2)}) copy-start(f32[2,384,2,128]{3,1,0,2:T(8,128)} %copy-done.1) | copy-start | bytes 2359300
  97.5 1.2 copy-start.5
  100.5 9.5 %all-to-all-start = ((bf16[4,96,256]{2,1,0:T(8,128)(2,1)}), bf16[4,96,256]{2,1,0:T(8,128)(2,1)S(1)}, u32[]{:S(2)}, u32[]{:S(2)}) async-start(bf16[4,96,256]{2,1,0:T(8,128)(2,1)} %multiply_convert_fusion.2), calls=%async_computation | async-start | bytes 393216 | tf_op jit(solution)/shard_map/all_to_all | solution.py:112
  103.9 102.5 %all-gather.8.cloned.1.call-start = ((), (), s32[]{:S(2)}) async-start(), calls=%async_computation.6 | async-start | bytes 4915200 | tf_op jit(solution)/shard_map/all_gather | solution.py:136
  110.4 4.1 %copy-start.8 = (f32[2048]{0:T(1024)S(1)}, f32[2048]{0:T(1024)}, u32[]{:S(2)}) copy-start(f32[2048]{0:T(1024)} %param.24) | copy-start | bytes 24580
  113.6 0.9 copy-start.3
  174.7 90.9 %reduce-scatter.2.cloned.1.call-start = ((), (), s32[]{:S(2)}) async-start(), calls=%async_computation.7 | async-start | bytes 4915200 | tf_op jit(solution)/shard_map/reduce_scatter | solution.py:142
  222.6 51.0 %copy-start.7 = (f32[96,2]{0,1:T(2,128)S(1)}, f32[96,2]{0,1:T(2,128)}, u32[]{:S(2)}) copy-start(f32[96,2]{0,1:T(2,128)} %param.26) | copy-start | bytes 2308
  268.0 31.3 %all-to-all-start.2 = ((bf16[8,30,2048]{2,1,0:T(8,128)(2,1)}), bf16[8,30,2048]{2,1,0:T(8,128)(2,1)}, u32[]{:S(2)}, u32[]{:S(2)}) async-start(bf16[8,30,2048]{2,1,0:T(8,128)(2,1)} %reshape.160), calls=%async_computation.3 | async-start | bytes 2097152 | tf_op jit(solution)/shard_map/all_to_all | solution.py:149
  302.9 6.8 %copy-start.4 = (f32[96,2048]{1,0:T(8,128)S(1)}, f32[96,2048]{1,0:T(8,128)}, u32[]{:S(2)}) copy-start(f32[96,2048]{1,0:T(8,128)} %copy-done.3) | copy-start | bytes 2359300
Sparse Core Ops, SparseCore 0:
  9.9 65.3 all-gather.3
  76.8 33.5 all-gather.5
  174.8 31.4 all-gather.7
  222.7 42.8 reduce-scatter.1
